TPU v7x, 32 devices: a whole 2x2x4 slice. The times are simulated.
32 devices in a mesh: grp: 2 (over y), fs: 4 (over z), tp: 4 (over x, core).
Axes of the slice: x: 2, y: 2, z: 4, core: 2. Of those that a mesh axis runs over, the one named last changes fastest.
Arguments:
- prompt: bfloat16 [1024, 2048], P(('grp', 'fs', 'tp')), parts along dimension 0, may hold values from -6 to 6
- norm_gain: float32 [2048], P('fs'), may hold values from 0.1 to 1.9
- up_weight: float32 [2048, 8192], P('fs', 'tp'), may hold values from -0.125 to 0.125
- down_weight: float32 [8192, 2048], P('fs', 'tp'), may hold values from -0.0625 to 0.0625
Outputs:
- up_serving: bfloat16 [4096, 8192], P('grp', 'fs'), parts along dimension 0
- down_serving: bfloat16 [8192, 4096], P('fs', 'grp'), parts along dimension 1
- mlp_output: bfloat16 [1024, 2048], P(('grp', 'fs', 'tp')), parts along dimension 0
There are 2 independent parts, one for each index of `grp`. A program takes and returns all parts, laid end to end along the dimension named above; an argument that names none is the same for every part. Nothing has to cross between parts.
All inputs are finite; a program needn't handle non-finite values.
Results may differ from a plain program's by a relative error of at most 0.024.
Values may be sent and summed in bfloat16 or wider, within the bound.
A program may use at most 128 MiB of HBM per device.

v0:
```python
import jax
import jax.numpy as jnp
from jax import lax
from jax.sharding import PartitionSpec as P

epsilon = 1e-06


def per_device(prompt, norm_gain, up_weight, down_weight):
    folded = (norm_gain[:, None] * up_weight).astype(jnp.bfloat16)
    down_local = down_weight.astype(jnp.bfloat16)
    down_serving = lax.all_gather(down_local, "tp", axis=1, tiled=True)
    thin_rows = lax.all_to_all(folded, "tp", split_axis=0, concat_axis=1, tiled=True)
    crossed = lax.all_to_all(thin_rows, "fs", split_axis=1, concat_axis=0, tiled=True)
    stacked = lax.all_gather(crossed, "tp", axis=0, tiled=True)
    tp_count = lax.axis_size("tp")
    fs_count = lax.axis_size("fs")
    slice_height = folded.shape[0] // tp_count
    unit_count = stacked.shape[1]
    up_serving = stacked.reshape(tp_count, fs_count, slice_height, unit_count)
    up_serving = up_serving.transpose(1, 0, 2, 3).reshape(-1, unit_count)
    widened = prompt.astype(jnp.float32)
    normed = (
        widened * lax.rsqrt(jnp.mean(widened * widened, axis=-1, keepdims=True) + epsilon)
    ).astype(jnp.bfloat16)
    projected = jnp.dot(
        lax.all_gather(normed, "fs", axis=0, tiled=True),
        up_serving,
        preferred_element_type=jnp.float32,
    )
    hidden = jnp.square(jax.nn.relu(projected)).astype(jnp.bfloat16)
    summed = lax.psum_scatter(
        jnp.dot(hidden, down_serving, preferred_element_type=jnp.float32).astype(jnp.bfloat16),
        "fs",
        scatter_dimension=0,
        tiled=True,
    )
    return (up_serving, down_serving, summed)


def solution(mesh):
    return jax.shard_map(
        per_device,
        mesh=mesh,
        in_specs=(P(("grp", "fs", "tp"), None), P("fs"), P("fs", "tp"), P("fs", "tp")),
        out_specs=(P("grp", "fs"), P("fs", "grp"), P(("grp", "fs", "tp"), None)),
        check_vma=False,
    )
```

profile of v0, /device:TPU:0, one launch (start us, length us, event | category | flops | bytes accessed | tf_op | source)
XLA Modules:
  0.0 255.5 jit_solution(17152566268026169703)
XLA Ops:
  7.2 0.0 all-gather.3.cloned.1.call-start
  7.2 2.5 multiply_convert_fusion
  9.7 29.7 %all_to_all.32 = bf16[4,128,2048]{2,1,0:T(8,128)(2,1)S(1)} all-to-all(bf16[4,128,2048]{2,1,0:T(8,128)(2,1)S(1)} %bitcast.17), channel_id=1, replica_groups=mesh['grp'=2,'fs'=4,'tp'=4] {'tp'}, dimensions={0} | all-to-all | bytes 4194304 | tf_op jit(solution)/shard_map/all_to_all | solution.py:13
  39.4 0.0 copy-start
  39.4 52.7 %all_to_all.33 = bf16[128,4,2048]{2,0,1:T(8,128)(2,1)} all-to-all(bf16[128,4,2048]{2,0,1:T(8,128)(2,1)S(1)} %bitcast.16), channel_id=1, replica_groups=mesh['grp'=2,'fs'=4,'tp'=4] {'fs'}, dimensions={1} | all-to-all | bytes 4194304 | tf_op jit(solution)/shard_map/all_to_all | solution.py:14
  92.1 0.0 all-gather.3.cloned.1.call-update
  92.1 0.0 all-gather.5.cloned.1.call-start
  92.2 3.8 %convert_element_type.19 = bf16[2048,512]{1,0:T(8,128)(2,1)} convert(f32[2048,512]{1,0:T(8,128)} %param.7) | non-fusion elementwise | flops 1048576 | bytes 6291456 | tf_op jit(solution)/shard_map/convert_element_type | solution.py:11
  96.0 0.0 all-gather.5.cloned.1.call-update
  96.0 0.0 reduce-scatter.2.cloned.1.call-start
  96.0 0.0 copy-done
  96.1 0.1 fusion.3
  96.2 0.1 fusion.4
  96.3 15.7 %all_gather.11 = bf16[128,2048]{1,0:T(8,128)(2,1)S(1)} all-gather(bf16[32,2048]{1,0:T(8,128)(2,1)S(1)} %fusion.4), channel_id=1, replica_groups=mesh['grp'=2,'fs'=4,'tp'=4] {'fs'}, dimensions={0}, use_global_device_ids=true | all-gather | bytes 655360 | tf_op jit(solution)/shard_map/all_gather | solution.py:27
  112.0 37.2 %all-gather.3.cloned.1.call-done = bf16[2048,2048]{1,0:T(8,128)(2,1)} async-done(((bf16[512,2048]{1,0:T(8,128)(2,1)}), bf16[2048,2048]{1,0:T(8,128)(2,1)}) %all-gather.3.cloned.1.call-update) | async-done | bytes 8388624 | tf_op jit(solution)/shard_map/all_gather | solution.py:15
  149.2 8.4 %copy.7 = bf16[4,4,128,2048]{3,2,1,0:T(8,128)(2,1)} copy(bf16[4,4,128,2048]{3,2,0,1:T(8,128)(2,1)} %bitcast.14) | data formatting | bytes 16777216 | tf_op jit(solution)/shard_map/transpose | solution.py:21
  157.6 52.0 %all-gather.5.cloned.1.call-done = bf16[2048,2048]{1,0:T(8,128)(2,1)} async-done(((bf16[2048,512]{1,0:T(8,128)(2,1)}), bf16[2048,2048]{1,0:T(8,128)(2,1)}) %all-gather.5.cloned.1.call-update) | async-done | bytes 8388624 | tf_op jit(solution)/shard_map/all_gather | solution.py:12
  209.6 8.9 %convolution_convert_fusion = bf16[128,2048]{1,0:T(8,128)(2,1)} fusion(bf16[2048,2048]{1,0:T(8,128)(2,1)} %all-gather.5.cloned.1.call-done, bf16[128,2048]{1,0:T(8,128)(2,1)S(1)} %all_gather.11, bf16[2048,2048]{1,0:T(8,128)(2,1)} %bitcast.12), kind=kOutput, calls=%fused_computation.3 | convolution fusion | flops 2148532224 | bytes 17825792 | tf_op jit(solution)/shard_map/dot_general | solution.py:33
  218.5 0.0 reduce-scatter.2.cloned.1.call-update
  218.5 22.0 %reduce-scatter.2.cloned.1.call-done = bf16[32,2048]{1,0:T(8,128)(2,1)} async-done(((bf16[128,2048]{1,0:T(8,128)(2,1)}), bf16[32,2048]{1,0:T(8,128)(2,1)}) %reduce-scatter.2.cloned.1.call-update) | async-done | bytes 131088 | tf_op jit(solution)/shard_map/reduce_scatter | solution.py:32
  240.5 8.4 %copy.9 = bf16[2048,2048]{1,0:T(8,128)(2,1)} copy(bf16[2048,2048]{1,0:T(8,128)(2,1)} %all-gather.5.cloned.1.call-done) | data formatting | bytes 16777216
  (1 shorter events, 0.0 us)
Async XLA Ops:
  7.2 142.0 %all-gather.3.cloned.1.call-start = ((), (), s32[]{:S(2)}) async-start(), calls=%async_computation.3 | async-start | bytes 10485760 | tf_op jit(solution)/shard_map/all_gather | solution.py:15
  39.4 56.7 %copy-start = (bf16[32,2048]{1,0:T(8,128)(2,1)S(1)}, bf16[32,2048]{1,0:T(8,128)(2,1)}, u32[]{:S(2)}) copy-start(bf16[32,2048]{1,0:T(8,128)(2,1)} %param.4) | copy-start | bytes 393220
  92.1 117.4 %all-gather.5.cloned.1.call-start = ((), (), s32[]{:S(2)}) async-start(), calls=%async_computation.4 | async-start | bytes 10485760 | tf_op jit(solution)/shard_map/all_gather | solution.py:12
  96.0 144.5 %reduce-scatter.2.cloned.1.call-start = ((), (), s32[]{:S(2)}) async-start(), calls=%async_computation.5 | async-start | bytes 655360 | tf_op jit(solution)/shard_map/reduce_scatter | solution.py:32
Sparse Core Ops, SparseCore 0:
  92.3 56.8 all-gather.2
  151.3 58.2 all-gather.4
  218.7 21.8 reduce-scatter.1
where the time goes:
time: 256 us; the launch traced here: 255 us
  waiting for transfers between devices  111 us (43%)
  blocking collectives  98.1 us (38%)
  local copies, waits for them, and re-layouts  16.9 us (7%)
  between operations  13.8 us (5%)
  matrix products  8.93 us (3%)
  other arithmetic  6.49 us (3%)
    all_to_all x1, blocking collectives, per_device(): lax.all_to_all(thin_rows, 'fs', split_axis=1, concat_axis=0, tiled=True)  52.7 us
    all_gather x1, waiting for transfers between devices, per_device(): down_serving = lax.all_gather(down_local, 'tp', axis=1, tiled=True)  52 us
    all_gather x1, waiting for transfers between devices, per_device(): stacked = lax.all_gather(crossed, 'tp', axis=0, tiled=True)  37.2 us
    all_to_all x1, blocking collectives, per_device(): lax.all_to_all(folded, 'tp', split_axis=0, concat_axis=1, tiled=True)  29.7 us
    reduce_scatter x1, waiting for transfers between devices, per_device(): lax.psum_scatter(jnp.dot(hidden, down_serving, preferred_element_type=jnp...  22 us
    all_gather x1, blocking collectives, per_device(): lax.all_gather(normed, 'fs', axis=0, tiled=True)  15.7 us
    dot_general x1, matrix products, per_device(): jnp.dot(hidden, down_serving, preferred_element_type=jnp.float32)  8.93 us
    unnamed x3, local copies, waits for them, and re-layouts  8.44 us
  transfers between devices with their start and end apart: 3, of which 3 were waited for; matrix products, arithmetic and copies ran while one was open for 5% of the time, Pallas kernels for 0%

commit v1 on v0

--- a/solution.py
+++ b/solution.py
@@ -9,7 +9,7 @@
 def per_device(prompt, norm_gain, up_weight, down_weight):
     folded = (norm_gain[:, None] * up_weight).astype(jnp.bfloat16)
     down_local = down_weight.astype(jnp.bfloat16)
-    down_serving = lax.all_gather(down_local, "tp", axis=1, tiled=True)
+    down_serving = jnp.concatenate(lax.all_gather(down_local, "tp"), axis=1)
     thin_rows = lax.all_to_all(folded, "tp", split_axis=0, concat_axis=1, tiled=True)
     crossed = lax.all_to_all(thin_rows, "fs", split_axis=1, concat_axis=0, tiled=True)
     stacked = lax.all_gather(crossed, "tp", axis=0, tiled=True)

time: 256 us -> 217 us (0.85)
  waiting for transfers between devices: 111 us -> 40.2 us
  blocking collectives: 98.1 us -> 116 us
  local copies, waits for them, and re-layouts: 16.9 us -> 31 us
    all_gather x1, waiting for transfers between devices: 52 us -> 0.01 us  [per_device(): down_serving = jnp.concatenate(lax.all_gather(down_local, 'tp'), axis=1)]
    all_gather x1, waiting for transfers between devices: 37.2 us -> 18.1 us  [per_device(): stacked = lax.all_gather(crossed, 'tp', axis=0, tiled=True)]
    all_to_all x1, blocking collectives: 29.7 us -> 48.1 us  [per_device(): lax.all_to_all(folded, 'tp', split_axis=0, concat_axis=1, tiled=True)]
    all_gather x0 -> x1, local copies, waits for them, and re-layouts: none -> 12.2 us  [per_device(): down_serving = jnp.concatenate(lax.all_gather(down_local, 'tp'), axis=1)]
    unnamed x3 -> x5, local copies, waits for them, and re-layouts: 8.44 us -> 10.4 us
  transfers between devices with their start and end apart: 3 -> 3, of which waited for: 3 -> 2; matrix products, arithmetic and copies ran while one was open for 5% -> 12% of each run, Pallas kernels for 0% -> 0%
where the time goes in v1:
time: 217 us
  blocking collectives  116 us (53%)
  waiting for transfers between devices  40.2 us (19%)
  local copies, waits for them, and re-layouts  31 us (14%)
  between operations  13.8 us (6%)
  matrix products  8.92 us (4%)
  other arithmetic  6.49 us (3%)
    all_to_all x1, blocking collectives, per_device(): lax.all_to_all(thin_rows, 'fs', split_axis=1, concat_axis=0, tiled=True)  52.6 us
    all_to_all x1, blocking collectives, per_device(): lax.all_to_all(folded, 'tp', split_axis=0, concat_axis=1, tiled=True)  48.1 us
    reduce_scatter x1, waiting for transfers between devices, per_device(): lax.psum_scatter(jnp.dot(hidden, down_serving, preferred_element_type=jnp...  22 us
    all_gather x1, waiting for transfers between devices, per_device(): stacked = lax.all_gather(crossed, 'tp', axis=0, tiled=True)  18.1 us
    all_gather x1, blocking collectives, per_device(): lax.all_gather(normed, 'fs', axis=0, tiled=True)  15.7 us
    all_gather x1, local copies, waits for them, and re-layouts, per_device(): down_serving = jnp.concatenate(lax.all_gather(down_local, 'tp'), axis=1)  12.2 us
    unnamed x5, local copies, waits for them, and re-layouts  10.4 us
    dot_general x1, matrix products, per_device(): jnp.dot(hidden, down_serving, preferred_element_type=jnp.float32)  8.92 us
  transfers between devices with their start and end apart: 3, of which 2 were waited for; matrix products, arithmetic and copies ran while one was open for 12% of the time, Pallas kernels for 0%

profile of v1, /device:TPU:0, one launch (start us, length us, event | category | flops | bytes accessed | tf_op | source)
XLA Modules:
  0.0 216.8 jit_solution(9657787762168556309)
XLA Ops:
  7.2 0.0 copy-start.1
  7.2 0.0 all-gather.6.cloned.1.call-start
  7.2 3.8 %convert_element_type.19 = bf16[2048,512]{1,0:T(8,128)(2,1)} convert(f32[2048,512]{1,0:T(8,128)} %param.7) | non-fusion elementwise | flops 1048576 | bytes 6291456 | tf_op jit(solution)/shard_map/convert_element_type | solution.py:11
  11.0 0.0 all-gather.6.cloned.1.call-update
  11.0 0.0 copy-start
  11.0 0.0 all-gather.4.cloned.1.call-start
  11.1 0.0 copy-done.1
  11.1 2.5 %multiply_convert_fusion = bf16[512,2048]{1,0:T(8,128)(2,1)S(1)} fusion(f32[512,2048]{1,0:T(8,128)} %param.6, f32[512]{0:T(512)S(1)} %copy-done.1), kind=kLoop, calls=%fused_computation | loop fusion | flops 2097152 | bytes 6293504 | tf_op jit(solution)/shard_map/convert_element_type | solution.py:10
  13.6 48.1 %all_to_all.32 = bf16[4,128,2048]{2,1,0:T(8,128)(2,1)S(1)} all-to-all(bf16[4,128,2048]{2,1,0:T(8,128)(2,1)S(1)} %bitcast.25), channel_id=1, replica_groups=mesh['grp'=2,'fs'=4,'tp'=4] {'tp'}, dimensions={0} | all-to-all | bytes 4194304 | tf_op jit(solution)/shard_map/all_to_all | solution.py:13
  61.6 52.6 %all_to_all.33 = bf16[128,4,2048]{2,0,1:T(8,128)(2,1)} all-to-all(bf16[128,4,2048]{2,0,1:T(8,128)(2,1)S(1)} %bitcast.24), channel_id=1, replica_groups=mesh['grp'=2,'fs'=4,'tp'=4] {'fs'}, dimensions={1} | all-to-all | bytes 4194304 | tf_op jit(solution)/shard_map/all_to_all | solution.py:14
  114.2 0.0 all-gather.4.cloned.1.call-update
  114.2 0.0 reduce-scatter.2.cloned.1.call-start
  114.3 0.0 copy-done
  114.3 0.1 fusion.3
  114.4 0.1 fusion.4
  114.5 15.7 %all_gather.15 = bf16[128,2048]{1,0:T(8,128)(2,1)S(1)} all-gather(bf16[32,2048]{1,0:T(8,128)(2,1)S(1)} %fusion.4), channel_id=1, replica_groups=mesh['grp'=2,'fs'=4,'tp'=4] {'fs'}, dimensions={0}, use_global_device_ids=true | all-gather | bytes 655360 | tf_op jit(solution)/shard_map/all_gather | solution.py:27
  130.2 0.0 all-gather.6.cloned.1.call-done
  130.2 12.2 %copy.10 = bf16[4,2048,512]{2,0,1:T(4,128)(2,1)} copy(bf16[4,2048,512]{2,1,0:T(8,128)(2,1)} %bitcast.21) | data formatting | bytes 16777216 | tf_op jit(solution)/shard_map/all_gather | solution.py:12
  142.4 10.4 %copy.11 = bf16[256,8,4,512]{3,1,2,0:T(8,128)(2,1)} copy(bf16[256,8,4,512]{3,2,1,0:T(4,128)(2,1)} %bitcast.20) | data formatting | bytes 16777216
  152.8 18.1 %all-gather.4.cloned.1.call-done = bf16[2048,2048]{1,0:T(8,128)(2,1)} async-done(((bf16[512,2048]{1,0:T(8,128)(2,1)}), bf16[2048,2048]{1,0:T(8,128)(2,1)}) %all-gather.4.cloned.1.call-update) | async-done | bytes 8388624 | tf_op jit(solution)/shard_map/all_gather | solution.py:15
  170.9 8.4 %copy.9 = bf16[4,4,128,2048]{3,2,1,0:T(8,128)(2,1)} copy(bf16[4,4,128,2048]{3,2,0,1:T(8,128)(2,1)} %bitcast.22) | data formatting | bytes 16777216 | tf_op jit(solution)/shard_map/transpose | solution.py:21
  179.3 8.9 %convolution_convert_fusion = bf16[128,2048]{1,0:T(8,128)(2,1)} fusion(bf16[2048,2048]{1,0:T(8,128)(2,1)} %bitcast.16, bf16[128,2048]{1,0:T(8,128)(2,1)S(1)} %all_gather.15, bf16[2048,2048]{1,0:T(8,128)(2,1)} %bitcast.18), kind=kOutput, calls=%fused_computation.3 | convolution fusion | flops 2148532224 | bytes 17825792 | tf_op jit(solution)/shard_map/dot_general | solution.py:33
  188.2 0.0 reduce-scatter.2.cloned.1.call-update
  188.3 22.0 %reduce-scatter.2.cloned.1.call-done = bf16[32,2048]{1,0:T(8,128)(2,1)} async-done(((bf16[128,2048]{1,0:T(8,128)(2,1)}), bf16[32,2048]{1,0:T(8,128)(2,1)}) %reduce-scatter.2.cloned.1.call-update) | async-done | bytes 131088 | tf_op jit(solution)/shard_map/reduce_scatter | solution.py:32
  (1 shorter events, 0.0 us)
Async XLA Ops:
  7.2 3.9 %copy-start.1 = (f32[512]{0:T(512)S(1)}, f32[512]{0:T(512)}, u32[]{:S(2)}) copy-start(f32[512]{0:T(512)} %param.5) | copy-start | bytes 6148
  7.2 123.0 %all-gather.6.cloned.1.call-start = ((), (), s32[]{:S(2)}) async-start(), calls=%async_computation.5 | async-start | bytes 10485760 | tf_op jit(solution)/shard_map/all_gather | solution.py:12
  11.0 103.3 %copy-start = (bf16[32,2048]{1,0:T(8,128)(2,1)S(1)}, bf16[32,2048]{1,0:T(8,128)(2,1)}, u32[]{:S(2)}) copy-start(bf16[32,2048]{1,0:T(8,128)(2,1)} %param.4) | copy-start | bytes 393220
  11.0 159.8 %all-gather.4.cloned.1.call-start = ((), (), s32[]{:S(2)}) async-start(), calls=%async_computation.3 | async-start | bytes 10485760 | tf_op jit(solution)/shard_map/all_gather | solution.py:15
  114.2 96.0 %reduce-scatter.2.cloned.1.call-start = ((), (), s32[]{:S(2)}) async-start(), calls=%async_computation.4 | async-start | bytes 655360 | tf_op jit(solution)/shard_map/reduce_scatter | solution.py:32
Sparse Core Ops, SparseCore 0:
  11.1 78.8 all-gather.5
  114.4 56.4 all-gather.3
  188.4 21.8 reduce-scatter.1

commit v2 on v0

--- a/solution.py
+++ b/solution.py
@@ -12,7 +12,9 @@
     down_serving = lax.all_gather(down_local, "tp", axis=1, tiled=True)
     thin_rows = lax.all_to_all(folded, "tp", split_axis=0, concat_axis=1, tiled=True)
     crossed = lax.all_to_all(thin_rows, "fs", split_axis=1, concat_axis=0, tiled=True)
-    stacked = lax.all_gather(crossed, "tp", axis=0, tiled=True)
+    stacked = jnp.concatenate(
+        lax.all_to_all(jnp.stack([crossed] * lax.axis_size("tp")), "tp", 0, 0), axis=0
+    )
     tp_count = lax.axis_size("tp")
     fs_count = lax.axis_size("fs")
     slice_height = folded.shape[0] // tp_count

time: 256 us -> 271 us (1.059)
  blocking collectives: 98.1 us -> 117 us
  waiting for transfers between devices: 111 us -> 96.8 us
  starting transfers between devices: 0.12 us -> 5.86 us
  local copies, waits for them, and re-layouts: 16.9 us -> 21.3 us
    all_to_all x0 -> x1, waiting for transfers between devices: none -> 76.6 us  [per_device(): lax.all_to_all(jnp.stack([crossed] * lax.axis_size('tp')), 'tp', 0, 0)]
    all_gather x1, waiting for transfers between devices: 52 us -> 0.01 us  [per_device(): down_serving = lax.all_gather(down_local, 'tp', axis=1, tiled=True)]
    all_gather x1 -> x0, waiting for transfers between devices: 37.2 us -> none  [per_device(): stacked = lax.all_gather(crossed, 'tp', axis=0, tiled=True)]
    all_to_all x1, blocking collectives: 29.7 us -> 48 us  [per_device(): lax.all_to_all(folded, 'tp', split_axis=0, concat_axis=1, tiled=True)]
    all_to_all x0 -> x1, starting transfers between devices: none -> 5.79 us  [per_device(): lax.all_to_all(jnp.stack([crossed] * lax.axis_size('tp')), 'tp', 0, 0)]
    another operation x0 -> x1, local copies, waits for them, and re-layouts: none -> 4.46 us  [per_device(): jnp.stack([crossed] * lax.axis_size('tp'))]
    unnamed x3 -> x5, local copies, waits for them, and re-layouts: 8.44 us -> 8.45 us
  transfers between devices with their start and end apart: 3 -> 3, of which waited for: 3 -> 2; matrix products, arithmetic and copies ran while one was open for 5% -> 6% of each run, Pallas kernels for 0% -> 0%
where the time goes in v2:
time: 271 us; the launch traced here: 270 us
  blocking collectives  117 us (43%)
  waiting for transfers between devices  96.8 us (36%)
  local copies, waits for them, and re-layouts  21.3 us (8%)
  between operations  14.1 us (5%)
  matrix products  8.93 us (3%)
  other arithmetic  6.49 us (2%)
  starting transfers between devices  5.86 us (2%)
    all_to_all x1, waiting for transfers between devices, per_device(): lax.all_to_all(jnp.stack([crossed] * lax.axis_size('tp')), 'tp', 0, 0)  76.6 us
    all_to_all x1, blocking collectives, per_device(): lax.all_to_all(thin_rows, 'fs', split_axis=1, concat_axis=0, tiled=True)  52.5 us
    all_to_all x1, blocking collectives, per_device(): lax.all_to_all(folded, 'tp', split_axis=0, concat_axis=1, tiled=True)  48 us
    reduce_scatter x1, waiting for transfers between devices, per_device(): lax.psum_scatter(jnp.dot(hidden, down_serving, preferred_element_type=jnp...  20.2 us
    all_gather x1, blocking collectives, per_device(): lax.all_gather(normed, 'fs', axis=0, tiled=True)  16.2 us
    dot_general x1, matrix products, per_device(): jnp.dot(hidden, down_serving, preferred_element_type=jnp.float32)  8.93 us
    unnamed x5, local copies, waits for them, and re-layouts  8.45 us
    transpose x1, local copies, waits for them, and re-layouts, per_device(): up_serving = up_serving.transpose(1, 0, 2, 3).reshape(-1, unit_count)  8.44 us
  transfers between devices with their start and end apart: 3, of which 2 were waited for; matrix products, arithmetic and copies ran while one was open for 6% of the time, Pallas kernels for 0%

profile of v2, /device:TPU:0, one launch (start us, length us, event | category | flops | bytes accessed | tf_op | source)
XLA Modules:
  0.0 270.3 jit_solution(8743239027570895288)
XLA Ops:
  7.2 0.0 copy-start.1
  7.2 0.0 all-gather.2.cloned.1.call-start
  7.2 3.8 %convert_element_type.19 = bf16[2048,512]{1,0:T(8,128)(2,1)} convert(f32[2048,512]{1,0:T(8,128)} %param.7) | non-fusion elementwise | flops 1048576 | bytes 6291456 | tf_op jit(solution)/shard_map/convert_element_type | solution.py:11
  11.0 0.0 all-gather.2.cloned.1.call-update
  11.0 0.0 copy-done.1
  11.0 2.5 multiply_convert_fusion
  13.5 48.0 %all_to_all.34 = bf16[4,128,2048]{2,1,0:T(8,128)(2,1)S(1)} all-to-all(bf16[4,128,2048]{2,1,0:T(8,128)(2,1)S(1)} %bitcast.16), channel_id=1, replica_groups=mesh['grp'=2,'fs'=4,'tp'=4] {'tp'}, dimensions={0} | all-to-all | bytes 4194304 | tf_op jit(solution)/shard_map/all_to_all | solution.py:13
  61.5 52.5 %all_to_all.35 = bf16[128,4,2048]{2,0,1:T(8,128)(2,1)S(1)} all-to-all(bf16[128,4,2048]{2,0,1:T(8,128)(2,1)S(1)} %bitcast.15), channel_id=1, replica_groups=mesh['grp'=2,'fs'=4,'tp'=4] {'fs'}, dimensions={1} | all-to-all | bytes 4194304 | tf_op jit(solution)/shard_map/all_to_all | solution.py:14
  114.0 4.5 %stack.10 = bf16[4,512,2048]{2,1,0:T(8,128)(2,1)} broadcast(bf16[512,2048]{1,0:T(8,128)(2,1)S(1)} %bitcast.14), dimensions={1,2} | broadcast | bytes 10485760 | tf_op jit(solution)/shard_map/stack | solution.py:16
  118.4 0.0 copy-start
  118.4 5.8 %all-to-all-start.2 = ((bf16[4,512,2048]{2,1,0:T(8,128)(2,1)}), bf16[4,512,2048]{2,1,0:T(8,128)(2,1)}, u32[]{:S(2)}, u32[]{:S(2)}) async-start(bf16[4,512,2048]{2,1,0:T(8,128)(2,1)} %stack.10), calls=%async_computation.2 | async-start | bytes 16777216 | tf_op jit(solution)/shard_map/all_to_all | solution.py:16
  124.2 0.0 reduce-scatter.2.cloned.1.call-start
  124.3 0.0 copy-done
  124.3 0.1 fusion.3
  124.5 0.1 fusion.4
  124.6 16.2 %all_gather.7 = bf16[128,2048]{1,0:T(8,128)(2,1)S(1)} all-gather(bf16[32,2048]{1,0:T(8,128)(2,1)S(1)} %fusion.4), channel_id=1, replica_groups=mesh['grp'=2,'fs'=4,'tp'=4] {'fs'}, dimensions={0}, use_global_device_ids=true | all-gather | bytes 655360 | tf_op jit(solution)/shard_map/all_gather | solution.py:29
  140.8 76.6 %all-to-all-done.2 = bf16[4,512,2048]{2,1,0:T(8,128)(2,1)} async-done(((bf16[4,512,2048]{2,1,0:T(8,128)(2,1)}), bf16[4,512,2048]{2,1,0:T(8,128)(2,1)}, u32[]{:S(2)}, u32[]{:S(2)}) %all-to-all-start.2) | async-done | bytes 8388640 | tf_op jit(solution)/shard_map/all_to_all | solution.py:16
  217.4 8.4 %copy.7 = bf16[4,4,128,2048]{3,2,1,0:T(8,128)(2,1)} copy(bf16[4,4,128,2048]{3,2,0,1:T(8,128)(2,1)} %bitcast.5) | data formatting | bytes 16777216 | tf_op jit(solution)/shard_map/transpose | solution.py:23
  225.8 0.0 all-gather.2.cloned.1.call-done
  225.8 8.9 %convolution_convert_fusion = bf16[128,2048]{1,0:T(8,128)(2,1)} fusion(bf16[2048,2048]{1,0:T(8,128)(2,1)} %all-gather.2.cloned.1.call-done, bf16[128,2048]{1,0:T(8,128)(2,1)S(1)} %all_gather.7, bf16[2048,2048]{1,0:T(8,128)(2,1)} %bitcast.12), kind=kOutput, calls=%fused_computation.3 | convolution fusion | flops 2148532224 | bytes 17825792 | tf_op jit(solution)/shard_map/dot_general | solution.py:35
  234.8 0.0 reduce-scatter.2.cloned.1.call-update
  234.8 20.2 %reduce-scatter.2.cloned.1.call-done = bf16[32,2048]{1,0:T(8,128)(2,1)} async-done(((bf16[128,2048]{1,0:T(8,128)(2,1)}), bf16[32,2048]{1,0:T(8,128)(2,1)}) %reduce-scatter.2.cloned.1.call-update) | async-done | bytes 131088 | tf_op jit(solution)/shard_map/reduce_scatter | solution.py:34
  255.0 8.4 %copy.9 = bf16[2048,2048]{1,0:T(8,128)(2,1)} copy(bf16[2048,2048]{1,0:T(8,128)(2,1)} %all-gather.2.cloned.1.call-done) | data formatting | bytes 16777216
  (1 shorter events, 0.0 us)
Async XLA Ops:
  7.2 3.9 %copy-start.1 = (f32[512]{0:T(512)S(1)}, f32[512]{0:T(512)}, u32[]{:S(2)}) copy-start(f32[512]{0:T(512)} %param.5) | copy-start | bytes 6148
  7.2 218.7 %all-gather.2.cloned.1.call-start = ((), (), s32[]{:S(2)}) async-start(), calls=%async_computation.4 | async-start | bytes 10485760 | tf_op jit(solution)/shard_map/all_gather | solution.py:12
  118.4 5.8 %copy-start = (bf16[32,2048]{1,0:T(8,128)(2,1)S(1)}, bf16[32,2048]{1,0:T(8,128)(2,1)}, u32[]{:S(2)}) copy-start(bf16[32,2048]{1,0:T(8,128)(2,1)} %param.4) | copy-start | bytes 393220
  118.4 98.9 %all-to-all-start.2 = ((bf16[4,512,2048]{2,1,0:T(8,128)(2,1)}), bf16[4,512,2048]{2,1,0:T(8,128)(2,1)}, u32[]{:S(2)}, u32[]{:S(2)}) async-start(bf16[4,512,2048]{2,1,0:T(8,128)(2,1)} %stack.10), calls=%async_computation.2 | async-start | bytes 16777216 | tf_op jit(solution)/shard_map/all_to_all | solution.py:16
  124.2 130.8 %reduce-scatter.2.cloned.1.call-start = ((), (), s32[]{:S(2)}) async-start(), calls=%async_computation.5 | async-start | bytes 655360 | tf_op jit(solution)/shard_map/reduce_scatter | solution.py:34
Sparse Core Ops, SparseCore 0:
  11.1 78.7 all-gather.1
  234.9 20.0 reduce-scatter.1
